TPU v7x, 32 devices: a whole 2x2x4 slice. The times are simulated.
32 devices in a mesh: ep: 8 (over z, y), tp: 4 (over x, core).
Axes of the slice: x: 2, y: 2, z: 4, core: 2. Of those that a mesh axis runs over, the one named last changes fastest.
Arguments:
- queries: bfloat16 [8192, 1024], P('ep', 'tp'), may hold values from -6 to 6
- key_rows: bfloat16 [8192, 256], P('ep', 'tp'), may hold values from -6 to 6
- values: bfloat16 [8192, 256], P('ep', 'tp'), may hold values from -6 to 6
- sink_logit: float32 [16], P('tp'), may hold values from 3 to 7
- out_weight: bfloat16 [1024, 2048], P('tp'), may hold values from -0.1875 to 0.1875
- out_gain: float32 [2048], replicated, may hold values from 0.1 to 1.9
- routed_tokens: bfloat16 [16384, 2048], P(('ep', 'tp')), may hold values from -6 to 6
- expert_ids: int32 [16384, 2], P(('ep', 'tp')), may hold values from 0 to 31, as said below
- route_weight: float32 [16384, 2], P(('ep', 'tp')), may hold values from 0.1 to 1
- routed_gain: float32 [2048], replicated, may hold values from 0.1 to 1.9
- expert_gate: bfloat16 [32, 2048, 1024], P('ep', None, 'tp'), may hold values from -0.125 to 0.125
- expert_up: bfloat16 [32, 2048, 1024], P('ep', None, 'tp'), may hold values from -0.125 to 0.125
- expert_down: bfloat16 [32, 2048, 1024], P('ep', None, 'tp'), may hold values from -0.1875 to 0.1875
Outputs:
- mixer_out: bfloat16 [8192, 2048], P(('ep', 'tp'))
- experts_out: bfloat16 [16384, 2048], P(('ep', 'tp'))
Inputs may be any that keep to these rules, and one draw needn't show every extreme that they name: `expert_ids`: both experts of a row lie in one group (equal id // 8); the 512 rows of one device name every group exactly 512 / 4 times; the rows of one device name no expert more than 64 times; in every device's rows some expert of each group is named exactly 64 times, and one expert is named exactly 64 times by the rows of every device.
All inputs are finite; a program needn't handle non-finite values.
Results may differ from a plain program's by a relative error of at most 0.0071.
Values may be sent and summed in bfloat16 or wider, within the bound.
A program may use at most 192 MiB of HBM per device.

v0:
```python
import functools

import jax
import jax.numpy as jnp
from jax import lax
from jax.experimental import pallas as pl
from jax.experimental.pallas import tpu as pltpu
from jax.sharding import Mesh, PartitionSpec as P

HEAD_DIM = 64
WINDOW = 128
QBLOCK = 512
EXPERTS = 32
EPG = 8
TOP = 2
GROUPS = EXPERTS // EPG
CHUNK_ROWS = 2048
ROW_TILE = 512

epsilon = 1e-06
EP = ("group", "member")
PLANE = ("member", "tp")


def padded(block, width):
    count = lax.axis_size(EP)
    forward = [(i, i + 1) for i in range(count - 1)]
    backward = [(target, source) for source, target in forward]
    low = lax.ppermute(block[-width:], EP, forward)
    high = lax.ppermute(block[:width], EP, backward)
    return jnp.concatenate([low, block, high], axis=0)


def attention(queries, key_rows, values, sink_logit):
    row_count = queries.shape[0]
    heads_here = queries.shape[1] // HEAD_DIM
    kv_here = key_rows.shape[1] // HEAD_DIM
    group_size = heads_here // kv_here
    paired = jnp.concatenate((key_rows, values), axis=1)
    extended = padded(paired, WINDOW)
    offset = lax.axis_index(EP) * row_count
    seq_total = row_count * lax.axis_size(EP)
    grouped = queries.reshape(row_count, kv_here, group_size, HEAD_DIM)
    sinks = sink_logit.reshape(kv_here, group_size)[:, :, None, None]
    span_keys = QBLOCK + 2 * WINDOW

    def attend_block(block_index):
        start_row = block_index * QBLOCK
        query_block = lax.dynamic_slice_in_dim(grouped, start_row, QBLOCK, 0)
        band = lax.dynamic_slice_in_dim(extended, start_row, span_keys, 0)
        key_block = band[:, : kv_here * HEAD_DIM].reshape(span_keys, kv_here, HEAD_DIM)
        value_block = band[:, kv_here * HEAD_DIM :].reshape(span_keys, kv_here, HEAD_DIM)
        scores = jnp.einsum(
            "qhgd,khd->hgqk", query_block, key_block, preferred_element_type=jnp.float32
        ) * HEAD_DIM ** (-0.5)
        query_pos = offset + start_row + jnp.arange(QBLOCK, dtype=jnp.int32)
        key_pos = offset + start_row - WINDOW + jnp.arange(span_keys, dtype=jnp.int32)
        valid = (
            (jnp.abs(key_pos[None, :] - query_pos[:, None]) <= WINDOW)
            & (key_pos[None, :] >= 0)
            & (key_pos[None, :] < seq_total)
        )
        masked = jnp.where(valid, scores, -1e30)
        largest = jnp.maximum(jnp.max(masked, axis=-1, keepdims=True), sinks)
        raised = jnp.where(valid, jnp.exp(masked - largest), 0.0)
        denominator = jnp.sum(raised, axis=-1, keepdims=True) + jnp.exp(sinks - largest)
        weights = (raised / denominator).astype(jnp.bfloat16)
        attended = jnp.einsum(
            "hgqk,khd->qhgd", weights, value_block, preferred_element_type=jnp.float32
        )
        return attended.astype(jnp.bfloat16).reshape(QBLOCK, heads_here * HEAD_DIM)

    attended = lax.map(attend_block, jnp.arange(row_count // QBLOCK, dtype=jnp.int32))
    attended = attended.reshape(row_count, heads_here * HEAD_DIM)
    return lax.all_to_all(attended, "tp", split_axis=0, concat_axis=1, tiled=True)


def project(attended, full_weight, out_gain):
    mixed = jnp.dot(attended, full_weight, preferred_element_type=jnp.float32)
    return (
        mixed * lax.rsqrt(jnp.mean(mixed * mixed, axis=-1, keepdims=True) + epsilon) * out_gain
    ).astype(jnp.bfloat16)


def expert_kernel(x_ref, w_ref, gate_ref, up_ref, down_ref, out_ref, total):
    x = x_ref[...]
    for e in range(gate_ref.shape[0]):
        gate = jnp.dot(x, gate_ref[e], preferred_element_type=jnp.float32)
        upward = jnp.dot(x, up_ref[e], preferred_element_type=jnp.float32)
        hidden = (gate / (1.0 + jnp.exp(-gate)) * upward * w_ref[:, e : e + 1]).astype(
            jnp.bfloat16
        )
        part = lax.dot_general(
            hidden, down_ref[e], (((1,), (1,)), ((), ())), preferred_element_type=jnp.float32
        )
        if e == 0:
            total[...] = part
        else:
            total[...] += part
    out_ref[...] = total[...].astype(jnp.bfloat16)


def apply_experts(rows, weights, gate, up, down):
    count, width = rows.shape
    local_experts, _, units = gate.shape
    tile = min(ROW_TILE, count)
    whole = lambda i: (0, 0, 0)
    return pl.pallas_call(
        expert_kernel,
        grid=(count // tile,),
        out_shape=jax.ShapeDtypeStruct((count, width), jnp.bfloat16),
        in_specs=[
            pl.BlockSpec((tile, width), lambda i: (i, 0)),
            pl.BlockSpec((tile, local_experts), lambda i: (i, 0)),
            pl.BlockSpec(gate.shape, whole, pipeline_mode=pl.Buffered(1)),
            pl.BlockSpec(up.shape, whole, pipeline_mode=pl.Buffered(1)),
            pl.BlockSpec(down.shape, whole, pipeline_mode=pl.Buffered(1)),
        ],
        out_specs=pl.BlockSpec((tile, width), lambda i: (i, 0)),
        scratch_shapes=[pltpu.VMEM((tile, width), jnp.float32)],
        compiler_params=pltpu.CompilerParams(vmem_limit_bytes=48 * 2**20),
        cost_estimate=pl.CostEstimate(
            flops=6 * count * width * local_experts * units,
            bytes_accessed=4 * count * width + 6 * local_experts * units * width,
            transcendentals=count * local_experts * units,
        ),
    )(rows, weights, gate, up, down)


def routed(tokens, expert_ids, route_weight, gain, gate, up, down, full_weight, attended):
    token_total, width = tokens.shape
    share = token_total // GROUPS
    plane = lax.axis_size(PLANE)
    local_experts = gate.shape[0]
    inputs = tokens.astype(jnp.float32)
    normed = (
        inputs * lax.rsqrt(jnp.mean(inputs * inputs, axis=-1, keepdims=True) + epsilon) * gain
    ).astype(jnp.bfloat16)
    group = expert_ids[:, 0] // EPG
    in_group = (group[:, None] == jnp.arange(GROUPS, dtype=jnp.int32)).astype(jnp.float32)
    index = jnp.arange(token_total, dtype=jnp.int32)
    before = (index[None, :] < index[:, None]).astype(jnp.float32)
    ranks = jnp.dot(before, in_group, preferred_element_type=jnp.float32)
    rank = jnp.sum(ranks * in_group, axis=1).astype(jnp.int32)
    position = group * share + rank
    order = (position[None, :] == index[:, None]).astype(jnp.bfloat16)
    back = (position[:, None] == index[None, :]).astype(jnp.bfloat16)
    ordered = jnp.dot(order, normed, preferred_element_type=jnp.float32).astype(jnp.bfloat16)
    member = jnp.arange(EPG, dtype=jnp.int32)
    spread = jnp.sum(
        jnp.where((expert_ids % EPG)[:, :, None] == member, route_weight[:, :, None], 0.0), axis=1
    )
    spread = jnp.dot(
        order.astype(jnp.float32), spread, precision=lax.Precision.HIGHEST,
        preferred_element_type=jnp.float32,
    )
    spread = spread.reshape(GROUPS, share, EPG).transpose(0, 2, 1).reshape(GROUPS, EPG * share)
    spread = lax.all_to_all(spread, "group", 0, 0, tiled=True)
    spread = lax.all_gather(spread, PLANE, axis=0, tiled=True)
    spread = spread.reshape(plane, GROUPS, EPG, share)
    mine = lax.dynamic_slice_in_dim(
        spread, lax.axis_index("member") * local_experts, local_experts, 2
    ).transpose(0, 1, 3, 2)
    piece = max(min(share, CHUNK_ROWS // (plane * GROUPS)), 16)
    ordered = ordered.reshape(GROUPS, share, width)
    mine, attended = lax.optimization_barrier((mine, attended))
    results = []
    for start in range(0, share, piece):
        sent = lax.all_to_all(ordered[:, start : start + piece], "group", 0, 0, tiled=True)
        sent = sent.reshape(GROUPS * piece, width)
        if start == 0:
            sent, full_weight = lax.optimization_barrier((sent, full_weight))
        rows = lax.all_gather(sent, PLANE, axis=0, tiled=True)
        weights = mine[:, :, start : start + piece].reshape(plane * GROUPS * piece, local_experts)
        partial = apply_experts(rows, weights, gate, up, down)
        summed = lax.psum_scatter(partial, PLANE, scatter_dimension=0, tiled=True)
        summed = summed.reshape(GROUPS, piece, width)
        results.append(lax.all_to_all(summed, "group", 0, 0, tiled=True))
    result = jnp.concatenate(results, axis=1).reshape(token_total, width)
    result = jnp.dot(back, result, preferred_element_type=jnp.float32).astype(jnp.bfloat16)
    return result, full_weight, attended


def local(queries, key_rows, values, sink_logit, out_weight, out_gain, routed_tokens,
          expert_ids, route_weight, routed_gain, expert_gate, expert_up, expert_down):
    full_weight = lax.all_gather(out_weight, "tp", axis=0, tiled=True)
    attended = attention(queries, key_rows, values, sink_logit)
    experts_out, full_weight, attended = routed(
        routed_tokens, expert_ids, route_weight, routed_gain, expert_gate, expert_up, expert_down,
        full_weight, attended,
    )
    mixer_out = project(attended, full_weight, out_gain)
    return (mixer_out, experts_out)


def solution(mesh):
    ep, tp = mesh.shape["ep"], mesh.shape["tp"]
    split = Mesh(mesh.devices.reshape(GROUPS, ep // GROUPS, tp), ("group", "member", "tp"))
    every = ("group", "member", "tp")
    placed = (
        P(EP, "tp"),
        P(EP, "tp"),
        P(EP, "tp"),
        P("tp"),
        P("tp", None),
        P(),
        P(every, None),
        P(every, None),
        P(every, None),
        P(),
        P(EP, None, "tp"),
        P(EP, None, "tp"),
        P(EP, None, "tp"),
    )
    return jax.shard_map(
        local,
        mesh=split,
        in_specs=placed,
        out_specs=(P(every, None), P(every, None)),
        check_vma=False,
    )
```

profile of v0, /device:TPU:8, one launch (start us, length us, event | category | flops | bytes accessed | tf_op | source)
XLA Modules:
  0.0 355.3 jit_solution(7483643094747249076)
XLA Ops:
  7.2 0.7 all-gather.5.cloned.1.call-update
  7.9 0.7 and_select_fusion.1
  8.7 0.3 fusion.24
  8.9 2.1 fusion.18
  11.0 3.0 convolution_convert_fusion.1
  14.0 0.1 fusion.38
  14.2 29.3 %all_to_all.51 = bf16[4,64,2048]{2,1,0:T(8,128)(2,1)} all-to-all(bf16[4,64,2048]{2,1,0:T(8,128)(2,1)S(1)} %get-tuple-element.118), channel_id=1, replica_groups=mesh['group'=4,'member'=2,'tp'=4] {'group'}, dimensions={0} | all-to-all | bytes 2097152 | tf_op jit(solution)/shard_map/all_to_all | solution.py:169
  43.6 28.1 %all_to_all.52 = bf16[4,64,2048]{2,1,0:T(8,128)(2,1)} all-to-all(bf16[4,64,2048]{2,1,0:T(8,128)(2,1)S(1)} %get-tuple-element.119), channel_id=1, replica_groups=mesh['group'=4,'member'=2,'tp'=4] {'group'}, dimensions={0} | all-to-all | bytes 2097152 | tf_op jit(solution)/shard_map/all_to_all | solution.py:169
  71.8 4.7 %collective-permute-start.1 = (bf16[128,128]{0,1:T(8,128)(2,1)S(1)}, bf16[128,128]{0,1:T(8,128)(2,1)S(1)}, u32[]{:S(2)}, u32[]{:S(2)}) collective-permute-start(bf16[128,128]{0,1:T(8,128)(2,1)S(1)} %get-tuple-element.121), channel_id=1, source_target_pairs={{4,0},{8,4},{12,8},{16,12},{20,16},{24,20},{28,24},{5,1},{9,5},{13... | collective-permute-start | bytes 98312 | tf_op jit(solution)/shard_map/ppermute | solution.py:30
  76.5 1.9 collective-permute-start
  78.5 1.2 fusion.25
  79.7 4.3 %all-to-all-start = ((f32[4,1,1024]{2,1,0:T(1,128)}), f32[4,1,1024]{2,1,0:T(1,128)S(1)}, u32[]{:S(2)}, u32[]{:S(2)}) async-start(f32[4,1,1024]{2,1,0:T(1,128)} %bitcast.15), calls=%async_computation | async-start | bytes 32768 | tf_op jit(solution)/shard_map/all_to_all | solution.py:158
  84.0 0.2 copy.38
  84.3 26.8 %while.12 = (s32[]{:T(128)}, bf16[2,512,256]{2,1,0:T(8,128)(2,1)}, s32[2]{0:T(128)S(1)}, bf16[1280,128]{0,1:T(8,128)(2,1)S(1)}, s32[]{:T(128)}, /*index=5*/bf16[...) while((s32[]{:T(128)}, bf16[2,512,256]{2,1,0:T(8,128)(2,1)}, ...), condition=%wide.region_5.6_spmd, body=%wide.region_2.5_spmd.sunk | while | flops 426778112 | bytes 47478112 | solution.py:73
  84.3 0.6 dynamic_slice.33
  85.6 0.8 fusion.52
  86.4 1.2 fusion.53
  87.7 2.6 copy-done.2
  90.3 1.5 fusion.54
  91.9 5.0 %fusion.55 = bf16[64,4,512]{2,0,1:T(8,128)(2,1)S(1)} fusion(f32[4,512]{1,0:T(4,128)S(1)} %exponential_add_fusion.2, f32[4,512]{1,0:T(4,128)S(1)} %broadcast_maximum_fusion.2, f32[768,512,4]{1,0,2:T(8,128)} %copy-done.2, pred[512,768]{0,1:T(8,128)(4,1)S(1)} %fusion.52, bf16[1280,128]{0,1:T(8,128)(2,1)S(1)} %get-tuple-element.210, s32[]{:T(128)S(6)} %select_n.102, ...), kind=kOutput, calls=%fused_computation.10.clone.1 | convolution fusion | flops 210894848 | bytes 7061512 | tf_op jit(solution)/shard_map/while/body/eval_jaxpr/hgqk,khd->qhgd/dot_general | solution.py:68
  96.9 0.1 copy.47
  97.0 0.7 constant_dynamic-update-slice_fusion.4
  97.7 0.6 dynamic_slice.33
  99.0 0.8 fusion.52
  99.8 1.2 fusion.53
  101.1 2.6 copy-done.2
  103.7 1.5 fusion.54
  105.3 4.9 %fusion.55 = bf16[64,4,512]{2,0,1:T(8,128)(2,1)S(1)} fusion(f32[4,512]{1,0:T(4,128)S(1)} %exponential_add_fusion.2, f32[4,512]{1,0:T(4,128)S(1)} %broadcast_maximum_fusion.2, f32[768,512,4]{1,0,2:T(8,128)} %copy-done.2, pred[512,768]{0,1:T(8,128)(4,1)S(1)} %fusion.52, bf16[1280,128]{0,1:T(8,128)(2,1)S(1)} %get-tuple-element.210, s32[]{:T(128)S(6)} %select_n.102, ...), kind=kOutput, calls=%fused_computation.10.clone.1 | convolution fusion | flops 210894848 | bytes 7061512 | tf_op jit(solution)/shard_map/while/body/eval_jaxpr/hgqk,khd->qhgd/dot_general | solution.py:68
  110.2 0.1 copy.47
  110.4 0.7 constant_dynamic-update-slice_fusion.4
  111.1 3.5 all-to-all-start.1
  114.7 20.1 %all-gather = f32[32,1,1024]{2,1,0:T(1,128)S(1)} all-gather(f32[4,1,1024]{2,1,0:T(1,128)S(1)} %all-to-all-done), channel_id=2, replica_groups=mesh['group'=4,'member'=2,'tp'=4] {'member','tp'}, dimensions={0}, use_global_device_ids=true | all-gather | bytes 147456 | tf_op jit(solution)/shard_map/all_gather | solution.py:159
  134.8 0.2 copy.40
  135.1 0.4 copy.42
  135.5 2.2 copy-done
  137.8 33.3 %shard_map.141 = bf16[2048,2048]{1,0:T(8,128)(2,1)} custom-call(bf16[2048,2048]{1,0:T(8,128)(2,1)} %all-gather.9.cloned.1.call-done.x_ref, f32[2048,4]{1,0:T(8,128)S(1)} %bitcast.91, bf16[4,2048,256]{2,1,0:T(8,128)(2,1)S(1)} %copy-done, bf16[4,2048,256]{2,1,0:T(8,128)(2,1)} %up_ref.3, bf16[4,2048,256]{2,1,0:T(8,128)(2,1)} %down_ref.3), custom_call_target="tpu_custom_call" | custom-call | flops 25769803776 | bytes 29360128 | tf_op jit(solution)/shard_map/pallas_call | solution.py:108
  171.1 0.4 copy.41
  171.6 2.2 copy-done.1
  173.8 32.9 %shard_map.140 = bf16[2048,2048]{1,0:T(8,128)(2,1)} custom-call(bf16[2048,2048]{1,0:T(8,128)(2,1)} %all-gather.7.cloned.1.call-done.x_ref, f32[2048,4]{1,0:T(8,128)S(1)} %bitcast.92, bf16[4,2048,256]{2,1,0:T(8,128)(2,1)S(1)} %copy-done.1, bf16[4,2048,256]{2,1,0:T(8,128)(2,1)} %up_ref.3, bf16[4,2048,256]{2,1,0:T(8,128)(2,1)} %down_ref.3), custom_call_target="tpu_custom_call" | custom-call | flops 25769803776 | bytes 29360128 | tf_op jit(solution)/shard_map/pallas_call | solution.py:108
  206.7 37.0 %reduce-scatter.5.cloned.1.call-done = bf16[256,2048]{1,0:T(8,128)(2,1)} async-done(((bf16[2048,2048]{1,0:T(8,128)(2,1)}), bf16[256,2048]{1,0:T(8,128)(2,1)}) %reduce-scatter.5.cloned.1.call-update) | async-done | bytes 1048592 | tf_op jit(solution)/shard_map/reduce_scatter | solution.py:176
  243.6 28.9 %all_to_all.53 = bf16[4,64,2048]{2,1,0:T(8,128)(2,1)S(1)} all-to-all(bf16[4,64,2048]{2,1,0:T(8,128)(2,1)} %bitcast.101), channel_id=1, replica_groups=mesh['group'=4,'member'=2,'tp'=4] {'group'}, dimensions={0} | all-to-all | bytes 2097152 | tf_op jit(solution)/shard_map/all_to_all | solution.py:178
  272.5 46.0 %reduce-scatter.3.cloned.1.call-done = bf16[256,2048]{1,0:T(8,128)(2,1)} async-done(((bf16[2048,2048]{1,0:T(8,128)(2,1)}), bf16[256,2048]{1,0:T(8,128)(2,1)}) %reduce-scatter.3.cloned.1.call-update) | async-done | bytes 1048592 | tf_op jit(solution)/shard_map/reduce_scatter | solution.py:176
  318.5 5.2 %all-to-all-start.3 = ((bf16[4,64,2048]{2,1,0:T(8,128)(2,1)}), bf16[4,64,2048]{2,1,0:T(8,128)(2,1)S(1)}, u32[]{:S(2)}, u32[]{:S(2)}) async-start(bf16[4,64,2048]{2,1,0:T(8,128)(2,1)} %bitcast.100), calls=%async_computation.4 | async-start | bytes 2097152 | tf_op jit(solution)/shard_map/all_to_all | solution.py:178
  323.7 3.5 multiply_reduce_fusion
  327.3 1.2 multiply_convert_fusion
  328.5 17.5 %all-to-all-done.3 = bf16[4,64,2048]{2,1,0:T(8,128)(2,1)S(1)} async-done(((bf16[4,64,2048]{2,1,0:T(8,128)(2,1)}), bf16[4,64,2048]{2,1,0:T(8,128)(2,1)S(1)}, u32[]{:S(2)}, u32[]{:S(2)}) %all-to-all-start.3) | async-done | bytes 1048608 | tf_op jit(solution)/shard_map/all_to_all | solution.py:178
  346.0 0.1 pad_maximum_fusion
  346.2 2.6 convolution_convert_fusion
  (60 shorter events, 1.0 us)
Async XLA Ops:
  7.2 64.5 %all-gather.5.cloned.1.call-start = ((), (), s32[]{:S(2)}) async-start(), calls=%async_computation.8 | async-start | bytes 5242880 | tf_op jit(solution)/shard_map/all_gather | solution.py:186
  7.9 127.6 %all-gather.9.cloned.1.call-start = ((), (), s32[]{:S(2)}) async-start(), calls=%async_computation.11 | async-start | bytes 9437184 | tf_op jit(solution)/shard_map/all_gather | solution.py:173
  14.2 57.5 %copy-start.4 = (bf16[1024,64]{0,1:T(8,128)(2,1)S(1)}, bf16[1024,64]{0,1:T(8,128)(2,1)}, u32[]{:S(2)}) copy-start(bf16[1024,64]{0,1:T(8,128)(2,1)} %param.16) | copy-start | bytes 393220
  14.2 57.5 %copy-start.5 = (bf16[1024,64]{0,1:T(8,128)(2,1)S(1)}, bf16[1024,64]{0,1:T(8,128)(2,1)}, u32[]{:S(2)}) copy-start(bf16[1024,64]{0,1:T(8,128)(2,1)} %param.17) | copy-start | bytes 393220
  14.2 64.2 %copy-start.7 = (s32[512,2]{0,1:T(2,128)S(1)}, s32[512,2]{0,1:T(2,128)}, u32[]{:S(2)}) copy-start(s32[512,2]{0,1:T(2,128)} %param.22) | copy-start | bytes 12292
  14.2 64.2 %copy-start.9 = (f32[512,2]{0,1:T(2,128)S(1)}, f32[512,2]{0,1:T(2,128)}, u32[]{:S(2)}) copy-start(f32[512,2]{0,1:T(2,128)} %param.23) | copy-start | bytes 12292
  14.2 69.8 %copy-start.3 = (bf16[1024,256]{1,0:T(8,128)(2,1)S(1)}, bf16[1024,256]{1,0:T(8,128)(2,1)}, u32[]{:S(2)}) copy-start(bf16[1024,256]{1,0:T(8,128)(2,1)} %param.15) | copy-start | bytes 1572868
  14.2 70.0 %copy-start.6 = (f32[4]{0:T(128)S(1)}, f32[4]{0:T(128)}, u32[]{:S(2)}) copy-start(f32[4]{0:T(128)} %param.18) | copy-start | bytes 52
  43.5 128.0 %all-gather.7.cloned.1.call-start = ((), (), s32[]{:S(2)}) async-start(), calls=%async_computation.9 | async-start | bytes 9437184 | tf_op jit(solution)/shard_map/all_gather | solution.py:173
  71.8 12.4 %collective-permute-start.1 = (bf16[128,128]{0,1:T(8,128)(2,1)S(1)}, bf16[128,128]{0,1:T(8,128)(2,1)S(1)}, u32[]{:S(2)}, u32[]{:S(2)}) collective-permute-start(bf16[128,128]{0,1:T(8,128)(2,1)S(1)} %get-tuple-element.121), channel_id=1, source_target_pairs={{4,0},{8,4},{12,8},{16,12},{20,16},{24,20},{28,24},{5,1},{9,5},{13... | collective-permute-start | bytes 98312 | tf_op jit(solution)/shard_map/ppermute | solution.py:30
  76.5 7.7 %collective-permute-start = (bf16[128,128]{0,1:T(8,128)(2,1)S(1)}, bf16[128,128]{0,1:T(8,128)(2,1)S(1)}, u32[]{:S(2)}, u32[]{:S(2)}) collective-permute-start(bf16[128,128]{0,1:T(8,128)(2,1)S(1)} %get-tuple-element.120), channel_id=1, source_target_pairs={{0,4},{4,8},{8,12},{12,16},{16,20},{20,24},{24,28},{1,5},{5,9},{9,... | collective-permute-start | bytes 98312 | tf_op jit(solution)/shard_map/ppermute | solution.py:29
  79.7 31.4 %all-to-all-start = ((f32[4,1,1024]{2,1,0:T(1,128)}), f32[4,1,1024]{2,1,0:T(1,128)S(1)}, u32[]{:S(2)}, u32[]{:S(2)}) async-start(f32[4,1,1024]{2,1,0:T(1,128)} %bitcast.15), calls=%async_computation | async-start | bytes 32768 | tf_op jit(solution)/shard_map/all_to_all | solution.py:158
  87.6 2.7 copy-start.2
  101.0 2.7 copy-start.2
  111.1 23.7 %all-to-all-start.1 = ((bf16[4,256,256]{2,1,0:T(8,128)(2,1)}), bf16[4,256,256]{2,1,0:T(8,128)(2,1)S(1)}, u32[]{:S(2)}, u32[]{:S(2)}) async-start(bf16[4,256,256]{2,1,0:T(8,128)(2,1)} %bitcast.20), calls=%async_computation.1 | async-start | bytes 1048576 | tf_op jit(solution)/shard_map/all_to_all | solution.py:75
  114.6 129.0 %reduce-scatter.5.cloned.1.call-start = ((), (), s32[]{:S(2)}) async-start(), calls=%async_computation.12 | async-start | bytes 9437184 | tf_op jit(solution)/shard_map/reduce_scatter | solution.py:176
  135.5 2.2 copy-start
  171.1 147.4 %reduce-scatter.3.cloned.1.call-start = ((), (), s32[]{:S(2)}) async-start(), calls=%async_computation.10 | async-start | bytes 9437184 | tf_op jit(solution)/shard_map/reduce_scatter | solution.py:176
  171.6 2.2 copy-start.1
  318.5 8.8 %copy-start.8 = (f32[2048]{0:T(1024)S(1)}, f32[2048]{0:T(1024)}, u32[]{:S(2)}) copy-start(f32[2048]{0:T(1024)} %param.20) | copy-start | bytes 24580
  318.5 27.5 %all-to-all-start.3 = ((bf16[4,64,2048]{2,1,0:T(8,128)(2,1)}), bf16[4,64,2048]{2,1,0:T(8,128)(2,1)S(1)}, u32[]{:S(2)}, u32[]{:S(2)}) async-start(bf16[4,64,2048]{2,1,0:T(8,128)(2,1)} %bitcast.100), calls=%async_computation.4 | async-start | bytes 2097152 | tf_op jit(solution)/shard_map/all_to_all | solution.py:178
Sparse Core Ops, SparseCore 0:
  9.5 35.5 all-gather.4
  47.1 55.3 all-gather.8
  104.3 59.2 all-gather.6
  171.2 72.3 reduce-scatter.4
  246.9 71.4 reduce-scatter.2
where the time goes:
time: 360 us; the launch traced here: 355 us
  blocking collectives  106 us (29%)
  waiting for transfers between devices  101 us (28%)
  Pallas kernels  66.2 us (18%)
  matrix products  23.1 us (6%)
  starting transfers between devices  19.8 us (6%)
  local copies, waits for them, and re-layouts  14.1 us (4%)
  between operations  14.1 us (4%)
  other arithmetic  9.2 us (3%)
    reduce_scatter x2, waiting for transfers between devices, routed(): summed = lax.psum_scatter(partial, PLANE, scatter_dimension=0, tiled=True)  82.9 us
    pallas_call x2, Pallas kernels, apply_experts(): pl.pallas_call(expert_kernel, grid=(count // tile,), out_shape=jax.ShapeD...  66.2 us
    all_to_all x2, blocking collectives, routed(): lax.all_to_all(ordered[:, start:start + piece], 'group', 0, 0, tiled=True)  57.4 us
    all_to_all x1, blocking collectives, routed(): results.append(lax.all_to_all(summed, 'group', 0, 0, tiled=True))  28.9 us
    all_gather x1, blocking collectives, routed(): spread = lax.all_gather(spread, PLANE, axis=0, tiled=True)  20.1 us
    all_to_all x1, waiting for transfers between devices, routed(): results.append(lax.all_to_all(summed, 'group', 0, 0, tiled=True))  17.5 us
    dot_general x2, matrix products, attend_block(): jnp.einsum('hgqk,khd->qhgd', weights, value_block, preferred_element_type...  9.9 us
  transfers between devices with their start and end apart: 10, of which 3 were waited for; matrix products, arithmetic and copies ran while one was open for 10% of the time, Pallas kernels for 19%

commit v1 on v0

--- a/solution.py
+++ b/solution.py
@@ -181,10 +181,358 @@
     return result, full_weight, attended
 
 
+MESH = pl.DeviceIdType.MESH
+QUAD = 4
+PART_ROWS = 64
+
+
+def fused_experts(steps, rows, ordered, spread, gate, up, down, out,
+                  xbuf, wraw, wcol, wg, wu, wd, hid, own, part, got1, got2, fin,
+                  send, recv, wsem, ssem):
+    plane, member, place = (lax.axis_index(a) for a in ("group", "member", "tp"))
+    experts, width, units = gate.shape
+    share = spread.shape[-1]
+    here = experts * units
+    blocks = 2 * experts
+    first = rows // 2
+
+    def device(dz=0, dx=0, dy=0, dcore=0):
+        z = (plane // 2 + dz // 2) % 2 * 2 + (plane % 2 + dz % 2) % 2
+        t = (place // 2 + dx) % 2 * 2 + (place % 2 + dcore) % 2
+        return (z, (member + dy) % 2, t)
+
+    def far(s):
+        return (s + s // GROUPS) % GROUPS
+
+    def slot(q, start=0, count=rows):
+        return pl.ds(pl.multiple_of(q * rows + start, 16), count)
+
+    def remote(src, dst, s, k, target):
+        return pltpu.make_async_remote_copy(
+            src_ref=src, dst_ref=dst, send_sem=send.at[s, k], recv_sem=recv.at[s, k],
+            device_id=target, device_id_type=MESH,
+        )
+
+    def tokens_of(s):
+        return pl.ds(pl.multiple_of(far(s) * share + s // GROUPS * rows, 16), rows)
+
+    def local_in(s):
+        return pltpu.make_async_copy(
+            ordered.at[tokens_of(s)], xbuf.at[s, slot(0)], recv.at[s, 0]
+        )
+
+    def dispatch(s):
+        return remote(ordered.at[tokens_of(s)], xbuf.at[s, slot(0)], s, 0, device(far(s)))
+
+    def to_x(s):
+        return remote(xbuf.at[s, slot(0)], xbuf.at[s, slot(1)], s, 1, device(dx=1))
+
+    def to_y(s):
+        return remote(xbuf.at[s, slot(0)], xbuf.at[s, slot(2)], s, 2, device(dy=1))
+
+    def pass_y(s):
+        return remote(
+            xbuf.at[s, slot(1, 0, first)], xbuf.at[s, slot(3, 0, first)], s, 3, device(dy=1)
+        )
+
+    def pass_x(s):
+        return remote(
+            xbuf.at[s, slot(2, first, rows - first)],
+            xbuf.at[s, slot(3, first, rows - first)], s, 4, device(dx=1),
+        )
+
+    def corner_x(s):
+        return remote(
+            part.at[s, slot(2, 0, first)], got1.at[s, pl.ds(0, first)], s, 5, device(dx=1)
+        )
+
+    def corner_y(s):
+        return remote(
+            part.at[s, slot(2, first, rows - first)], got1.at[s, pl.ds(first, rows - first)],
+            s, 6, device(dy=1),
+        )
+
+    def sum_x(s):
+        return remote(part.at[s, slot(0)], got2.at[s, slot(0)], s, 7, device(dx=1))
+
+    def sum_y(s):
+        return remote(part.at[s, slot(1)], got2.at[s, slot(1)], s, 8, device(dy=1))
+
+    def give_back(s):
+        return remote(fin.at[s], out.at[tokens_of(s)], s, 9, device(far(s)))
+
+    def local_out(s):
+        return pltpu.make_async_copy(fin.at[s], out.at[tokens_of(s)], recv.at[s, 9])
+
+    def weight_refs(e, to):
+        at = to * experts + e
+        return (
+            (gate.at[e], wg.at[at]),
+            (up.at[e], wu.at[at]),
+            (down.at[e], wd.at[:, pl.ds(at * units, units)]),
+        )
+
+    def weight_copies():
+        for e in range(experts):
+            for n, (src, dst) in enumerate(weight_refs(e, 0)):
+                yield pltpu.make_async_copy(src, dst, wsem.at[0, 3 * e + n])
+            for n, (src, dst) in enumerate(weight_refs(e, 1)):
+                yield pltpu.make_async_remote_copy(
+                    src_ref=src, dst_ref=dst, send_sem=wsem.at[1, 3 * e + n],
+                    recv_sem=wsem.at[2, 3 * e + n], device_id=device(dcore=1),
+                    device_id_type=MESH,
+                )
+
+    def spread_copies():
+        for dz in range(GROUPS):
+            for q in range(QUAD):
+                dx, dy = q % 2, q // 2
+                src, dst, n = spread.at[dy, dz], wraw.at[dz, q], dz * QUAD + q
+                if n == 0:
+                    yield pltpu.make_async_copy(src, dst, ssem.at[1, n])
+                else:
+                    yield pltpu.make_async_remote_copy(
+                        src_ref=src, dst_ref=dst, send_sem=ssem.at[0, n], recv_sem=ssem.at[1, n],
+                        device_id=device(dz, dx, dy), device_id_type=MESH,
+                    )
+
+    barrier = pltpu.get_barrier_semaphore()
+    peers = [(z, q % 2, q // 2, 0) for z in range(GROUPS) for q in range(QUAD)][1:] + [(0, 0, 0, 1)]
+    for peer in peers:
+        pl.semaphore_signal(barrier, inc=1, device_id=device(*peer), device_id_type=MESH)
+    pl.semaphore_wait(barrier, len(peers))
+
+    for s in range(steps):
+        if far(s) == 0:
+            local_in(s).start()
+    for s in range(steps):
+        if far(s) != 0:
+            dispatch(s).start()
+    for copy in spread_copies():
+        copy.start()
+    for copy in weight_copies():
+        copy.start()
+
+    def gather(s):
+        @pl.when(far(s) == 0)
+        def _():
+            local_in(s).wait()
+
+        @pl.when(far(s) != 0)
+        def _():
+            dispatch(s).wait_recv()
+
+        to_x(s).start()
+        to_y(s).start()
+
+    def forward(s):
+        to_x(s).wait_recv()
+        pass_y(s).start()
+        to_y(s).wait_recv()
+        pass_x(s).start()
+
+    gather(0)
+    gather(1)
+    forward(0)
+
+    for copy in spread_copies():
+        if hasattr(copy, "wait_recv") and copy.is_remote:
+            copy.wait_recv()
+        else:
+            copy.wait()
+    for dz in range(GROUPS):
+        for q in range(QUAD):
+            turned = wraw[dz, q].T
+            for piece in range(share // rows):
+                s = piece * GROUPS + (dz - piece) % GROUPS
+                wcol[s, q * rows : (q + 1) * rows, :] = turned[piece * rows : (piece + 1) * rows]
+    for copy in weight_copies():
+        if copy.is_remote:
+            copy.wait_recv()
+        else:
+            copy.wait()
+
+    def compute(s):
+        for j in range(blocks):
+            x = xbuf[s]
+            g = jnp.dot(x, wg[j], preferred_element_type=jnp.float32)
+            u = jnp.dot(x, wu[j], preferred_element_type=jnp.float32)
+            e = j % experts
+            h = g / (1.0 + jnp.exp(-g)) * u * wcol[s, :, e : e + 1]
+            hid[:, j * units : (j + 1) * units] = h.astype(jnp.bfloat16)
+        step = 256
+
+        @pl.loop(0, width // step)
+        def _(n):
+            columns = pl.ds(pl.multiple_of(n * step, step), step)
+            p = lax.dot_general(
+                hid[...], wd[columns, :], (((1,), (1,)), ((), ())),
+                preferred_element_type=jnp.float32,
+            )
+            own[s % 3, :, columns] = p[:rows]
+            part[s, :, columns] = p[rows:].astype(jnp.bfloat16)
+
+    def settle(s):
+        corner_x(s).wait_recv()
+        held = part[s, rows : rows + first].astype(jnp.float32)
+        part[s, rows : rows + first] = (
+            held + got1[s, :first].astype(jnp.float32)
+        ).astype(jnp.bfloat16)
+        sum_y(s).start()
+        corner_y(s).wait_recv()
+        held = part[s, first:rows].astype(jnp.float32)
+        part[s, first:rows] = (held + got1[s, first:].astype(jnp.float32)).astype(jnp.bfloat16)
+        sum_x(s).start()
+
+    def finish(s):
+        sum_y(s).wait_recv()
+        sum_x(s).wait_recv()
+        fin[s] = (
+            own[s % 3] + got2[s, :rows].astype(jnp.float32) + got2[s, rows:].astype(jnp.float32)
+        ).astype(jnp.bfloat16)
+
+        @pl.when(far(s) == 0)
+        def _():
+            local_out(s).start()
+
+        @pl.when(far(s) != 0)
+        def _():
+            give_back(s).start()
+
+    @pl.loop(0, steps + 2)
+    def _(i):
+        @pl.when(i + 2 < steps)
+        def _():
+            gather(i + 2)
+
+        @pl.when(i + 1 < steps)
+        def _():
+            forward(i + 1)
+
+        @pl.when(i >= 2)
+        def _():
+            finish(i - 2)
+
+        @pl.when(i < steps)
+        def _():
+            pass_y(i).wait_recv()
+            pass_x(i).wait_recv()
+            compute(i)
+            corner_x(i).start()
+            corner_y(i).start()
+
+        @pl.when(jnp.logical_and(i >= 1, i < steps + 1))
+        def _():
+            settle(i - 1)
+
+    for copy in spread_copies():
+        if copy.is_remote:
+            copy.wait_send()
+    for copy in weight_copies():
+        if copy.is_remote:
+            copy.wait_send()
+
+    @pl.loop(0, steps)
+    def _(s):
+        for copy in (to_x, to_y, pass_y, pass_x, corner_x, corner_y, sum_x, sum_y):
+            copy(s).wait_send()
+
+        @pl.when(far(s) == 0)
+        def _():
+            local_out(s).wait()
+
+        @pl.when(far(s) != 0)
+        def _():
+            dispatch(s).wait_send()
+            give_back(s).wait()
+
+
+def apply_fused(ordered, spread, gate, up, down):
+    total, width = ordered.shape
+    experts, _, units = gate.shape
+    share = total // GROUPS
+    rows = min(PART_ROWS, share)
+    steps = total // rows
+    hidden = 2 * experts * units
+    anywhere = pl.BlockSpec(memory_space=pl.ANY)
+    dma = pltpu.SemaphoreType.DMA
+    return pl.pallas_call(
+        functools.partial(fused_experts, steps, rows),
+        out_shape=jax.ShapeDtypeStruct((total, width), jnp.bfloat16),
+        in_specs=[anywhere] * 5,
+        out_specs=anywhere,
+        scratch_shapes=[
+            pltpu.VMEM((steps, QUAD * rows, width), jnp.bfloat16),
+            pltpu.VMEM((GROUPS, QUAD) + spread.shape[-2:], jnp.float32),
+            pltpu.VMEM((steps, QUAD * rows, EPG), jnp.float32),
+            pltpu.VMEM((2 * experts, width, units), jnp.bfloat16),
+            pltpu.VMEM((2 * experts, width, units), jnp.bfloat16),
+            pltpu.VMEM((width, hidden), jnp.bfloat16),
+            pltpu.VMEM((QUAD * rows, hidden), jnp.bfloat16),
+            pltpu.VMEM((3, rows, width), jnp.float32),
+            pltpu.VMEM((steps, (QUAD - 1) * rows, width), jnp.bfloat16),
+            pltpu.VMEM((steps, rows, width), jnp.bfloat16),
+            pltpu.VMEM((steps, 2 * rows, width), jnp.bfloat16),
+            pltpu.VMEM((steps, rows, width), jnp.bfloat16),
+            dma((steps, 10)),
+            dma((steps, 10)),
+            dma((3, 3 * experts)),
+            dma((2, GROUPS * QUAD)),
+        ],
+        compiler_params=pltpu.CompilerParams(
+            collective_id=0, has_side_effects=True, vmem_limit_bytes=66 * 10**6
+        ),
+        cost_estimate=pl.CostEstimate(
+            flops=6 * QUAD * total * width * hidden,
+            bytes_accessed=6 * experts * units * width,
+            transcendentals=QUAD * total * hidden,
+        ),
+    )(ordered, spread, gate, up, down)
+
+
+def routed_fused(tokens, expert_ids, route_weight, gain, gate, up, down):
+    token_total, width = tokens.shape
+    share = token_total // GROUPS
+    local_experts = gate.shape[0]
+    inputs = tokens.astype(jnp.float32)
+    normed = (
+        inputs * lax.rsqrt(jnp.mean(inputs * inputs, axis=-1, keepdims=True) + epsilon) * gain
+    ).astype(jnp.bfloat16)
+    group = jnp.bitwise_xor(expert_ids[:, 0] // EPG, lax.axis_index("group"))
+    in_group = (group[:, None] == jnp.arange(GROUPS, dtype=jnp.int32)).astype(jnp.float32)
+    index = jnp.arange(token_total, dtype=jnp.int32)
+    before = (index[None, :] < index[:, None]).astype(jnp.float32)
+    ranks = jnp.dot(before, in_group, preferred_element_type=jnp.float32)
+    rank = jnp.sum(ranks * in_group, axis=1).astype(jnp.int32)
+    position = group * share + rank
+    order = (position[None, :] == index[:, None]).astype(jnp.bfloat16)
+    back = (position[:, None] == index[None, :]).astype(jnp.bfloat16)
+    ordered = jnp.dot(order, normed, preferred_element_type=jnp.float32).astype(jnp.bfloat16)
+    start = lax.axis_index("member") * local_experts
+    member = (jnp.arange(EPG, dtype=jnp.int32) + start) % EPG
+    spread = jnp.sum(
+        jnp.where((expert_ids % EPG)[:, :, None] == member, route_weight[:, :, None], 0.0), axis=1
+    )
+    spread = jnp.dot(
+        order.astype(jnp.float32), spread, precision=lax.Precision.HIGHEST,
+        preferred_element_type=jnp.float32,
+    )
+    spread = spread.reshape(GROUPS, share, EPG).transpose(0, 2, 1)
+    spread = jnp.stack([spread, jnp.roll(spread, local_experts, axis=1)])
+    result = apply_fused(ordered, spread, gate, up, down)
+    return jnp.dot(back, result, preferred_element_type=jnp.float32).astype(jnp.bfloat16)
+
+
 def local(queries, key_rows, values, sink_logit, out_weight, out_gain, routed_tokens,
           expert_ids, route_weight, routed_gain, expert_gate, expert_up, expert_down):
     full_weight = lax.all_gather(out_weight, "tp", axis=0, tiled=True)
     attended = attention(queries, key_rows, values, sink_logit)
+    if lax.axis_size("member") == 2 and lax.axis_size("tp") == 4:
+        experts_out = routed_fused(
+            routed_tokens, expert_ids, route_weight, routed_gain, expert_gate, expert_up,
+            expert_down,
+        )
+        return (project(attended, full_weight, out_gain), experts_out)
     experts_out, full_weight, attended = routed(
         routed_tokens, expert_ids, route_weight, routed_gain, expert_gate, expert_up, expert_down,
         full_weight, attended,

time: 360 us -> 270 us (0.75)
  Pallas kernels: 66.2 us -> 194 us
  blocking collectives: 106 us -> 0 us
  waiting for transfers between devices: 101 us -> 4.37 us
  starting transfers between devices: 19.8 us -> 9.57 us
    pallas_call x2 -> x1, Pallas kernels: 66.2 us -> 194 us  [apply_fused(): pl.pallas_call(functools.partial(fused_experts, steps, rows), out_shape=j...]
    all_to_all x3 -> x0, blocking collectives: 86.2 us -> none  [the longest x2 57.4 us: routed(): lax.all_to_all(ordered[:, start:start + piece], 'group', 0, 0, tiled=True)]
    reduce_scatter x2 -> x0, waiting for transfers between devices: 82.9 us -> none  [routed(): summed = lax.psum_scatter(partial, PLANE, scatter_dimension=0, tiled=True)]
    all_gather x1 -> x0, blocking collectives: 20.1 us -> none  [routed(): spread = lax.all_gather(spread, PLANE, axis=0, tiled=True)]
    all_to_all x2 -> x0, waiting for transfers between devices: 17.5 us -> none  [the longest x1 17.5 us: routed(): results.append(lax.all_to_all(summed, 'group', 0, 0, tiled=True))]
    all_to_all x2 -> x0, starting transfers between devices: 9.52 us -> none  [the longest x1 5.25 us: routed(): results.append(lax.all_to_all(summed, 'group', 0, 0, tiled=True))]
    all_to_all x1, waiting for transfers between devices: 0.01 us -> 4.33 us  [attention(): lax.all_to_all(attended, 'tp', split_axis=0, concat_axis=1, tiled=True)]
  transfers between devices with their start and end apart: 10 -> 4, of which waited for: 3 -> 1; matrix products, arithmetic and copies ran while one was open for 10% -> 12% of each run, Pallas kernels for 19% -> 72%
where the time goes in v1:
time: 270 us; the launch traced here: 269 us
  Pallas kernels  194 us (72%)
  matrix products  23.7 us (9%)
  between operations  14.3 us (5%)
  other arithmetic  11.2 us (4%)
  local copies, waits for them, and re-layouts  10.6 us (4%)
  starting transfers between devices  9.57 us (4%)
  waiting for transfers between devices  4.37 us (2%)
    pallas_call x1, Pallas kernels, apply_fused(): pl.pallas_call(functools.partial(fused_experts, steps, rows), out_shape=j...  194 us
    dot_general x2, matrix products, attend_block(): jnp.einsum('hgqk,khd->qhgd', weights, value_block, preferred_element_type...  9.85 us
  transfers between devices with their start and end apart: 4, of which 1 were waited for; matrix products, arithmetic and copies ran while one was open for 12% of the time, Pallas kernels for 72%

profile of v1, /device:TPU:8, one launch (start us, length us, event | category | flops | bytes accessed | tf_op | source)
XLA Modules:
  0.0 268.7 jit_solution(9814514880856201059)
XLA Ops:
  7.2 0.0 copy-start.1
  7.2 0.0 all-gather.2.cloned.1.call-start
  7.2 1.1 constant_dynamic-update-slice_fusion.2
  8.3 0.9 constant_dynamic-update-slice_fusion.1
  9.2 3.3 %collective-permute-start.1 = (bf16[128,128]{0,1:T(8,128)(2,1)S(1)}, bf16[128,128]{0,1:T(8,128)(2,1)S(1)}, u32[]{:S(2)}, u32[]{:S(2)}) collective-permute-start(bf16[128,128]{0,1:T(8,128)(2,1)S(1)} %get-tuple-element.111), channel_id=1, source_target_pairs={{4,0},{8,4},{12,8},{16,12},{20,16},{24,20},{28,24},{5,1},{9,5},{13... | collective-permute-start | bytes 98312 | tf_op jit(solution)/shard_map/ppermute | solution.py:30
  12.5 2.5 collective-permute-start
  15.1 0.0 all-gather.2.cloned.1.call-update
  15.1 2.1 fusion.18
  17.2 0.7 and_select_fusion
  17.9 0.7 fusion.38
  18.6 0.3 fusion.24
  18.9 0.8 select_reduce_fusion
  19.7 0.6 fusion.25
  20.3 0.0 copy-done.1
  20.4 2.8 %convolution_convert_fusion.1.ordered = bf16[512,2048]{1,0:T(8,128)(2,1)} fusion(bf16[512,2048]{1,0:T(8,128)(2,1)S(1)} %copy-done.1, f32[2048]{0:T(1024)S(1)} %copy-done.5, f32[512]{0:T(512)S(1)} %add_rsqrt_fusion, s32[512]{0:T(512)S(1)} %fusion.37), kind=kOutput, calls=%fused_computation.33 | convolution fusion | flops 1079246848 | bytes 4206592 | tf_op jit(solution)/shard_map/dot_general | solution.py:510
  23.1 0.6 pad_maximum_fusion.1.spread
  23.7 193.7 %shard_map.140 = bf16[512,2048]{1,0:T(8,128)(2,1)} custom-call(bf16[512,2048]{1,0:T(8,128)(2,1)} %convolution_convert_fusion.1.ordered, f32[2,4,8,128]{3,2,1,0:T(8,128)} %pad_maximum_fusion.1.spread, bf16[4,2048,256]{2,1,0:T(8,128)(2,1)} %gate.1, bf16[4,2048,256]{2,1,0:T(8,128)(2,1)} %up.1, bf16[4,2048,256]{2,1,0:T(8,128)(2,1)} %down.1), custom_call_target="tpu_custom_call" | custom-call | flops 51539607552 | bytes 12582912 | tf_op jit(solution)/shard_map/pallas_call | solution.py:459
  217.5 0.2 copy.26
  217.7 0.0 collective-permute-done.1
  217.7 0.0 collective-permute-done
  217.8 26.9 %while.12 = (s32[]{:T(128)}, bf16[2,512,256]{2,1,0:T(8,128)(2,1)}, s32[2]{0:T(128)S(1)}, bf16[1280,128]{0,1:T(8,128)(2,1)S(1)}, s32[]{:T(128)}, /*index=5*/bf16[...) while((s32[]{:T(128)}, bf16[2,512,256]{2,1,0:T(8,128)(2,1)}, ...), condition=%wide.region_3.4_spmd, body=%wide.region_0.3_spmd.sunk | while | flops 426778112 | bytes 47478112 | solution.py:73
  217.8 0.7 dynamic_slice.28
  219.1 0.8 fusion.54
  219.9 1.2 fusion.55
  221.1 0.1 broadcast_maximum_fusion.2
  221.2 2.6 copy-done
  223.8 1.6 fusion.56
  225.3 0.1 exponential_add_fusion.2
  225.4 4.9 %fusion.57 = bf16[64,4,512]{2,0,1:T(8,128)(2,1)S(1)} fusion(f32[4,512]{1,0:T(4,128)S(1)} %exponential_add_fusion.2, f32[4,512]{1,0:T(4,128)S(1)} %broadcast_maximum_fusion.2, f32[768,512,4]{1,0,2:T(8,128)} %copy-done, pred[512,768]{0,1:T(8,128)(4,1)S(1)} %fusion.54, bf16[1280,128]{0,1:T(8,128)(2,1)S(1)} %get-tuple-element.200, s32[]{:T(128)S(6)} %select_n.114, ...), kind=kOutput, calls=%fused_computation.10.clone.1 | convolution fusion | flops 210894848 | bytes 7061512 | tf_op jit(solution)/shard_map/while/body/eval_jaxpr/hgqk,khd->qhgd/dot_general | solution.py:68
  230.3 0.1 copy.33
  230.5 0.7 constant_dynamic-update-slice_fusion.4
  231.2 0.6 dynamic_slice.28
  232.5 0.8 fusion.54
  233.3 1.2 fusion.55
  234.6 0.1 broadcast_maximum_fusion.2
  234.6 2.6 copy-done
  237.2 1.6 fusion.56
  238.8 0.1 exponential_add_fusion.2
  238.8 4.9 %fusion.57 = bf16[64,4,512]{2,0,1:T(8,128)(2,1)S(1)} fusion(f32[4,512]{1,0:T(4,128)S(1)} %exponential_add_fusion.2, f32[4,512]{1,0:T(4,128)S(1)} %broadcast_maximum_fusion.2, f32[768,512,4]{1,0,2:T(8,128)} %copy-done, pred[512,768]{0,1:T(8,128)(4,1)S(1)} %fusion.54, bf16[1280,128]{0,1:T(8,128)(2,1)S(1)} %get-tuple-element.200, s32[]{:T(128)S(6)} %select_n.114, ...), kind=kOutput, calls=%fused_computation.10.clone.1 | convolution fusion | flops 210894848 | bytes 7061512 | tf_op jit(solution)/shard_map/while/body/eval_jaxpr/hgqk,khd->qhgd/dot_general | solution.py:68
  243.8 0.1 copy.33
  243.9 0.7 constant_dynamic-update-slice_fusion.4
  244.6 3.7 %all-to-all-start = ((bf16[4,256,256]{2,1,0:T(8,128)(2,1)}), bf16[4,256,256]{2,1,0:T(8,128)(2,1)S(1)}, u32[]{:S(2)}, u32[]{:S(2)}) async-start(bf16[4,256,256]{2,1,0:T(8,128)(2,1)} %bitcast.13), calls=%async_computation | async-start | bytes 1048576 | tf_op jit(solution)/shard_map/all_to_all | solution.py:75
  248.3 4.2 %convolution_convert_fusion = bf16[512,2048]{1,0:T(8,128)(2,1)} fusion(bf16[512,2048]{1,0:T(8,128)(2,1)} %shard_map.140, s32[512]{0:T(512)S(1)} %bitcast.94), kind=kOutput, calls=%fused_computation.32 | convolution fusion | flops 1075052544 | bytes 4196352 | tf_op jit(solution)/shard_map/dot_general | solution.py:523
  252.5 4.3 %all-to-all-done = bf16[4,256,256]{2,1,0:T(8,128)(2,1)S(1)} async-done(((bf16[4,256,256]{2,1,0:T(8,128)(2,1)}), bf16[4,256,256]{2,1,0:T(8,128)(2,1)S(1)}, u32[]{:S(2)}, u32[]{:S(2)}) %all-to-all-start) | async-done | bytes 524320 | tf_op jit(solution)/shard_map/all_to_all | solution.py:75
  256.9 0.2 copy.28
  257.1 0.0 all-gather.2.cloned.1.call-done
  257.1 3.5 %multiply_reduce_fusion = (f32[256]{0:T(256)S(1)}, f32[256,2048]{1,0:T(8,128)S(1)}) fusion(bf16[256,1024]{0,1:T(8,128)(2,1)S(1)} %bitcast.85, bf16[1024,2048]{1,0:T(8,128)(2,1)} %all-gather.2.cloned.1.call-done), kind=kOutput, calls=%fused_computation.37 | convolution fusion | flops 1074790144 | bytes 6816768 | tf_op jit(solution)/shard_map/dot_general | solution.py:79
  260.7 1.2 multiply_convert_fusion
  (29 shorter events, 0.2 us)
Async XLA Ops:
  7.2 13.2 %copy-start.1 = (bf16[512,2048]{1,0:T(8,128)(2,1)S(1)}, bf16[512,2048]{1,0:T(8,128)(2,1)}, u32[]{:S(2)}) copy-start(bf16[512,2048]{1,0:T(8,128)(2,1)} %param.21) | copy-start | bytes 6291460
  7.2 13.2 %copy-start.5 = (f32[2048]{0:T(1024)S(1)}, f32[2048]{0:T(1024)}, u32[]{:S(2)}) copy-start(f32[2048]{0:T(1024)} %param.24) | copy-start | bytes 24580
  7.2 249.9 %all-gather.2.cloned.1.call-start = ((), (), s32[]{:S(2)}) async-start(), calls=%async_computation.1 | async-start | bytes 5242880 | tf_op jit(solution)/shard_map/all_gather | solution.py:528
  9.2 208.5 %collective-permute-start.1 = (bf16[128,128]{0,1:T(8,128)(2,1)S(1)}, bf16[128,128]{0,1:T(8,128)(2,1)S(1)}, u32[]{:S(2)}, u32[]{:S(2)}) collective-permute-start(bf16[128,128]{0,1:T(8,128)(2,1)S(1)} %get-tuple-element.111), channel_id=1, source_target_pairs={{4,0},{8,4},{12,8},{16,12},{20,16},{24,20},{28,24},{5,1},{9,5},{13... | collective-permute-start | bytes 98312 | tf_op jit(solution)/shard_map/ppermute | solution.py:30
  12.5 205.1 %collective-permute-start = (bf16[128,128]{0,1:T(8,128)(2,1)S(1)}, bf16[128,128]{0,1:T(8,128)(2,1)S(1)}, u32[]{:S(2)}, u32[]{:S(2)}) collective-permute-start(bf16[128,128]{0,1:T(8,128)(2,1)S(1)} %get-tuple-element.110), channel_id=1, source_target_pairs={{0,4},{4,8},{8,12},{12,16},{16,20},{20,24},{24,28},{1,5},{5,9},{9,... | collective-permute-start | bytes 98312 | tf_op jit(solution)/shard_map/ppermute | solution.py:29
  23.7 193.7 %copy-start.2 = (bf16[1024,256]{1,0:T(8,128)(2,1)S(1)}, bf16[1024,256]{1,0:T(8,128)(2,1)}, u32[]{:S(2)}) copy-start(bf16[1024,256]{1,0:T(8,128)(2,1)} %param.15) | copy-start | bytes 1572868
  23.7 194.0 %copy-start.3 = (f32[4]{0:T(128)S(1)}, f32[4]{0:T(128)}, u32[]{:S(2)}) copy-start(f32[4]{0:T(128)} %param.18) | copy-start | bytes 52
  221.1 2.6 copy-start
  234.5 2.6 copy-start
  244.6 12.3 %all-to-all-start = ((bf16[4,256,256]{2,1,0:T(8,128)(2,1)}), bf16[4,256,256]{2,1,0:T(8,128)(2,1)S(1)}, u32[]{:S(2)}, u32[]{:S(2)}) async-start(bf16[4,256,256]{2,1,0:T(8,128)(2,1)} %bitcast.13), calls=%async_computation | async-start | bytes 1048576 | tf_op jit(solution)/shard_map/all_to_all | solution.py:75
  252.5 8.1 %copy-start.4 = (f32[2048]{0:T(1024)S(1)}, f32[2048]{0:T(1024)}, u32[]{:S(2)}) copy-start(f32[2048]{0:T(1024)} %param.20) | copy-start | bytes 24580
Sparse Core Ops, SparseCore 0:
  15.2 49.8 all-gather.1

commit v2 on v1

--- a/solution.py
+++ b/solution.py
@@ -186,15 +186,23 @@
 PART_ROWS = 64
 
 
-def fused_experts(steps, rows, ordered, spread, gate, up, down, out,
-                  xbuf, wraw, wcol, wg, wu, wd, hid, own, part, got1, got2, fin,
-                  send, recv, wsem, ssem):
+def fused_layer(steps, rows, ordered, spread, gate, up, down, queries, pairs, sinks, out_weight,
+                out_gain, out, mixer_out,
+                xbuf, wraw, wcol, wg, wu, wd, hid, own, part, got1, got2, fin,
+                held_queries, band, mine, theirs, wo, mixed, stage,
+                send, recv, wsem, ssem, asem):
     plane, member, place = (lax.axis_index(a) for a in ("group", "member", "tp"))
     experts, width, units = gate.shape
     share = spread.shape[-1]
     here = experts * units
     blocks = 2 * experts
     first = rows // 2
+    sequence_rows = queries.shape[0]
+    heads_here = queries.shape[1] // HEAD_DIM
+    lanes = 2 * HEAD_DIM
+    token_rows = mixed.shape[0]
+    ep_count = GROUPS * 2
+    ep_place = plane * 2 + member
 
     def device(dz=0, dx=0, dy=0, dcore=0):
         z = (plane // 2 + dz // 2) % 2 * 2 + (plane % 2 + dz % 2) % 2
@@ -296,8 +304,115 @@
                         device_id=device(dz, dx, dy), device_id_type=MESH,
                     )
 
+    def attention_remote(src, dst, n, target):
+        return pltpu.make_async_remote_copy(
+            src_ref=src, dst_ref=dst, send_sem=asem.at[0, n], recv_sem=asem.at[1, n],
+            device_id=target, device_id_type=MESH,
+        )
+
+    def along_ep(distance):
+        to = (ep_place + ep_count + distance) % ep_count
+        return (to // 2, to % 2, place)
+
+    band_low = attention_remote(
+        pairs.at[pl.ds(sequence_rows - WINDOW, WINDOW)], band.at[pl.ds(0, WINDOW)], 0, along_ep(1)
+    )
+    band_high = attention_remote(
+        pairs.at[pl.ds(0, WINDOW)], band.at[pl.ds(WINDOW + sequence_rows, WINDOW)], 1,
+        along_ep(-1),
+    )
+    band_own = pltpu.make_async_copy(pairs, band.at[pl.ds(WINDOW, sequence_rows)], asem.at[2, 0])
+    queries_in = pltpu.make_async_copy(queries, held_queries, asem.at[2, 1])
+    wo_own = pltpu.make_async_copy(out_weight, wo.at[0], asem.at[2, 2])
+    wo_core = attention_remote(out_weight, wo.at[1], 2, device(dcore=1))
+    wo_across = attention_remote(out_weight, wo.at[2], 3, device(dx=1))
+    wo_pass = attention_remote(wo.at[2], wo.at[3], 4, device(dcore=1))
+
+    def attended_to(k):
+        dx, dcore = k // 2, k % 2
+        to = device(dx=dx, dcore=dcore)
+        start = pl.multiple_of(to[2] * token_rows, 16)
+        return attention_remote(
+            mine.at[pl.ds(start, token_rows)], theirs.at[k - 1], 4 + k, to
+        )
+
+    mixer_done = pltpu.make_async_copy(stage, mixer_out, asem.at[2, 3])
+
+    def attend(b):
+        query_rows = WINDOW
+        span = 3 * WINDOW
+        start = pl.multiple_of(b * query_rows, 16)
+        held_band = band[pl.ds(start, span)]
+        low = lax.broadcasted_iota(jnp.int32, (span, lanes), 1) < HEAD_DIM
+        zero = jnp.zeros((span, lanes), jnp.bfloat16)
+        kv, vk = held_band[:, :lanes], held_band[:, lanes:]
+        keys = (jnp.where(low, kv, zero), jnp.where(low, zero, vk))
+        vals = (jnp.where(low, vk, zero), jnp.where(low, zero, kv))
+        row = lax.broadcasted_iota(jnp.int32, (query_rows, span), 0)
+        column = lax.broadcasted_iota(jnp.int32, (query_rows, span), 1)
+        key_pos = ep_place * sequence_rows + b * query_rows - WINDOW + column
+        valid = (
+            (column >= row) & (column <= row + 2 * WINDOW)
+            & (key_pos >= 0) & (key_pos < ep_count * sequence_rows)
+        )
+        for pair in range(heads_here // 2):
+            query_block = held_queries[
+                pl.ds(start, query_rows), pair * lanes : (pair + 1) * lanes
+            ]
+            total = None
+            for side in range(2):
+                scores = lax.dot_general(
+                    query_block, keys[side], (((1,), (1,)), ((), ())),
+                    preferred_element_type=jnp.float32,
+                ) * HEAD_DIM ** (-0.5)
+                sink = jnp.full((1, 1), sinks[pair * 2 + side], jnp.float32)
+                masked = jnp.where(valid, scores, -1e30)
+                largest = jnp.maximum(jnp.max(masked, axis=-1, keepdims=True), sink)
+                raised = jnp.where(valid, jnp.exp(masked - largest), 0.0)
+                denominator = jnp.sum(raised, axis=-1, keepdims=True) + jnp.exp(sink - largest)
+                weights = (raised / denominator).astype(jnp.bfloat16)
+                product = jnp.dot(weights, vals[side], preferred_element_type=jnp.float32)
+                total = product if total is None else total + product
+            mine[pl.ds(start, query_rows), pair * lanes : (pair + 1) * lanes] = total.astype(
+                jnp.bfloat16
+            )
+
+    def project_rows():
+        for k in range(1, 4):
+            attended_to(k).wait_recv()
+        wo_own.wait()
+        wo_core.wait_recv()
+        wo_pass.wait_recv()
+        start = pl.multiple_of(place * token_rows, 16)
+        step = 256
+
+        @pl.loop(0, width // step)
+        def _(n):
+            columns = pl.ds(pl.multiple_of(n * step, step), step)
+            total = jnp.dot(
+                mine[pl.ds(start, token_rows)], wo[0, :, columns],
+                preferred_element_type=jnp.float32,
+            )
+            for k in range(1, 4):
+                total = total + jnp.dot(
+                    theirs[k - 1], wo[k, :, columns], preferred_element_type=jnp.float32
+                )
+            mixed[:, columns] = total
+
+        piece = 32
+
+        @pl.loop(0, token_rows // piece)
+        def _(n):
+            chosen = pl.ds(pl.multiple_of(n * piece, piece), piece)
+            block = mixed[chosen]
+            scale = lax.rsqrt(jnp.mean(block * block, axis=-1, keepdims=True) + epsilon)
+            stage[chosen] = (block * scale * out_gain[...]).astype(jnp.bfloat16)
+
+        mixer_done.start()
+
     barrier = pltpu.get_barrier_semaphore()
-    peers = [(z, q % 2, q // 2, 0) for z in range(GROUPS) for q in range(QUAD)][1:] + [(0, 0, 0, 1)]
+    peers = [(z, q % 2, q // 2, 0) for z in range(GROUPS) for q in range(QUAD)][1:]
+    peers += [(0, 0, 0, 1), (0, 1, 0, 1)]
     for peer in peers:
         pl.semaphore_signal(barrier, inc=1, device_id=device(*peer), device_id_type=MESH)
     pl.semaphore_wait(barrier, len(peers))
@@ -308,9 +423,13 @@
     for s in range(steps):
         if far(s) != 0:
             dispatch(s).start()
+    for copy in (band_low, band_high, band_own, queries_in):
+        copy.start()
     for copy in spread_copies():
         copy.start()
     for copy in weight_copies():
+        copy.start()
+    for copy in (wo_own, wo_core, wo_across):
         copy.start()
 
     def gather(s):
@@ -332,8 +451,31 @@
         pass_x(s).start()
 
     gather(0)
-    gather(1)
-    forward(0)
+    band_own.wait()
+    queries_in.wait()
+    band_low.wait_recv()
+    band_high.wait_recv()
+    blocks_here = sequence_rows // WINDOW
+    turns = (blocks_here // 4, blocks_here * 5 // 8)
+
+    @pl.loop(0, blocks_here)
+    def _(b):
+        @pl.when(b == turns[0])
+        def _():
+            forward(0)
+            gather(1)
+
+        @pl.when(b == turns[1])
+        def _():
+            forward(1)
+            gather(2)
+
+        attend(b)
+
+    for k in range(1, 4):
+        attended_to(k).start()
+    wo_across.wait_recv()
+    wo_pass.start()
 
     for copy in spread_copies():
         if hasattr(copy, "wait_recv") and copy.is_remote:
@@ -403,11 +545,11 @@
     def _(i):
         @pl.when(i + 2 < steps)
         def _():
-            gather(i + 2)
-
-        @pl.when(i + 1 < steps)
-        def _():
-            forward(i + 1)
+            forward(i + 2)
+
+        @pl.when(i + 3 < steps)
+        def _():
+            gather(i + 3)
 
         @pl.when(i >= 2)
         def _():
@@ -425,6 +567,15 @@
         def _():
             settle(i - 1)
 
+        @pl.when(i == steps // 2)
+        def _():
+            project_rows()
+
+    mixer_done.wait()
+    for k in range(1, 4):
+        attended_to(k).wait_send()
+    for copy in (band_low, band_high, wo_core, wo_across, wo_pass):
+        copy.wait_send()
     for copy in spread_copies():
         if copy.is_remote:
             copy.wait_send()
@@ -447,20 +598,27 @@
             give_back(s).wait()
 
 
-def apply_fused(ordered, spread, gate, up, down):
+def apply_fused(ordered, spread, gate, up, down, queries, pairs, sinks, out_weight, out_gain):
     total, width = ordered.shape
     experts, _, units = gate.shape
     share = total // GROUPS
     rows = min(PART_ROWS, share)
     steps = total // rows
     hidden = 2 * experts * units
+    sequence_rows, head_columns = queries.shape
+    token_rows = sequence_rows // 4
     anywhere = pl.BlockSpec(memory_space=pl.ANY)
+    vector = pl.BlockSpec(memory_space=pltpu.VMEM)
+    scalar = pl.BlockSpec(memory_space=pltpu.SMEM)
     dma = pltpu.SemaphoreType.DMA
     return pl.pallas_call(
-        functools.partial(fused_experts, steps, rows),
-        out_shape=jax.ShapeDtypeStruct((total, width), jnp.bfloat16),
-        in_specs=[anywhere] * 5,
-        out_specs=anywhere,
+        functools.partial(fused_layer, steps, rows),
+        out_shape=(
+            jax.ShapeDtypeStruct((total, width), jnp.bfloat16),
+            jax.ShapeDtypeStruct((token_rows, width), jnp.bfloat16),
+        ),
+        in_specs=[anywhere] * 7 + [scalar, anywhere, vector],
+        out_specs=(anywhere, anywhere),
         scratch_shapes=[
             pltpu.VMEM((steps, QUAD * rows, width), jnp.bfloat16),
             pltpu.VMEM((GROUPS, QUAD) + spread.shape[-2:], jnp.float32),
@@ -474,10 +632,18 @@
             pltpu.VMEM((steps, rows, width), jnp.bfloat16),
             pltpu.VMEM((steps, 2 * rows, width), jnp.bfloat16),
             pltpu.VMEM((steps, rows, width), jnp.bfloat16),
+            pltpu.VMEM(queries.shape, jnp.bfloat16),
+            pltpu.VMEM((sequence_rows + 2 * WINDOW, pairs.shape[1]), jnp.bfloat16),
+            pltpu.VMEM(queries.shape, jnp.bfloat16),
+            pltpu.VMEM((3, token_rows, head_columns), jnp.bfloat16),
+            pltpu.VMEM((4,) + out_weight.shape, jnp.bfloat16),
+            pltpu.VMEM((token_rows, width), jnp.float32),
+            pltpu.VMEM((token_rows, width), jnp.bfloat16),
             dma((steps, 10)),
             dma((steps, 10)),
             dma((3, 3 * experts)),
             dma((2, GROUPS * QUAD)),
+            dma((3, 8)),
         ],
         compiler_params=pltpu.CompilerParams(
             collective_id=0, has_side_effects=True, vmem_limit_bytes=66 * 10**6
@@ -487,10 +653,11 @@
             bytes_accessed=6 * experts * units * width,
             transcendentals=QUAD * total * hidden,
         ),
-    )(ordered, spread, gate, up, down)
-
-
-def routed_fused(tokens, expert_ids, route_weight, gain, gate, up, down):
+    )(ordered, spread, gate, up, down, queries, pairs, sinks, out_weight, out_gain)
+
+
+def layer_fused(queries, key_rows, values, sink_logit, out_weight, out_gain, tokens, expert_ids,
+                route_weight, gain, gate, up, down):
     token_total, width = tokens.shape
     share = token_total // GROUPS
     local_experts = gate.shape[0]
@@ -519,20 +686,34 @@
     )
     spread = spread.reshape(GROUPS, share, EPG).transpose(0, 2, 1)
     spread = jnp.stack([spread, jnp.roll(spread, local_experts, axis=1)])
-    result = apply_fused(ordered, spread, gate, up, down)
-    return jnp.dot(back, result, preferred_element_type=jnp.float32).astype(jnp.bfloat16)
+    pairs = jnp.concatenate([key_rows, values, values, key_rows], axis=1)
+    result, mixer_out = apply_fused(
+        ordered, spread, gate, up, down, queries, pairs, sink_logit, out_weight,
+        out_gain.reshape(1, width),
+    )
+    result = jnp.dot(back, result, preferred_element_type=jnp.float32).astype(jnp.bfloat16)
+    return (mixer_out, result)
+
+
+def can_fuse(queries, key_rows):
+    return (
+        lax.axis_size("group") == GROUPS
+        and lax.axis_size("member") == 2
+        and lax.axis_size("tp") == 4
+        and key_rows.shape[1] == HEAD_DIM
+        and queries.shape[1] % (2 * HEAD_DIM) == 0
+    )
 
 
 def local(queries, key_rows, values, sink_logit, out_weight, out_gain, routed_tokens,
           expert_ids, route_weight, routed_gain, expert_gate, expert_up, expert_down):
+    if can_fuse(queries, key_rows):
+        return layer_fused(
+            queries, key_rows, values, sink_logit, out_weight, out_gain, routed_tokens,
+            expert_ids, route_weight, routed_gain, expert_gate, expert_up, expert_down,
+        )
     full_weight = lax.all_gather(out_weight, "tp", axis=0, tiled=True)
     attended = attention(queries, key_rows, values, sink_logit)
-    if lax.axis_size("member") == 2 and lax.axis_size("tp") == 4:
-        experts_out = routed_fused(
-            routed_tokens, expert_ids, route_weight, routed_gain, expert_gate, expert_up,
-            expert_down,
-        )
-        return (project(attended, full_weight, out_gain), experts_out)
     experts_out, full_weight, attended = routed(
         routed_tokens, expert_ids, route_weight, routed_gain, expert_gate, expert_up, expert_down,
         full_weight, attended,

time: 270 us -> 230 us (0.85)
  Pallas kernels: 194 us -> 216 us
  matrix products: 23.7 us -> 7.94 us
  between operations: 14.3 us -> 0.8 us
  starting transfers between devices: 9.57 us -> 0 us
  local copies, waits for them, and re-layouts: 10.6 us -> 1.35 us
  other arithmetic: 11.2 us -> 4.16 us
  waiting for transfers between devices: 4.37 us -> 0 us
    pallas_call x1, Pallas kernels: 194 us -> 216 us  [apply_fused(): pl.pallas_call(functools.partial(fused_layer, steps, rows), out_shape=(ja...]
    dot_general x9 -> x4, matrix products: 23.7 us -> 7.94 us  [the longest x1 4.3 us: layer_fused(): jnp.dot(back, result, preferred_element_type=jnp.float32)]
    ppermute x2 -> x0, starting transfers between devices: 5.84 us -> none  [the longest x1 3.31 us: padded(): high = lax.ppermute(block[:width], EP, backward)]
    while x4 -> x0, local copies, waits for them, and re-layouts: 5.13 us -> none
    all_to_all x1 -> x0, waiting for transfers between devices: 4.33 us -> none  [attention(): lax.all_to_all(attended, 'tp', split_axis=0, concat_axis=1, tiled=True)]
    all_to_all x1 -> x0, starting transfers between devices: 3.69 us -> none  [attention(): lax.all_to_all(attended, 'tp', split_axis=0, concat_axis=1, tiled=True)]
    reduce_sum x4 -> x2, other arithmetic: 5.97 us -> 2.3 us  [the longest x1 2.23 us: layer_fused(): jnp.mean(inputs * inputs, axis=-1, keepdims=True) + epsilon]
  transfers between devices with their start and end apart: 4 -> 0, of which waited for: 1 -> 0; matrix products, arithmetic and copies ran while one was open for 12% -> 0% of each run, Pallas kernels for 72% -> 0%
where the time goes in v2:
time: 230 us
  Pallas kernels  216 us (94%)
  matrix products  7.94 us (3%)
  other arithmetic  4.16 us (2%)
    pallas_call x1, Pallas kernels, apply_fused(): pl.pallas_call(functools.partial(fused_layer, steps, rows), out_shape=(ja...  216 us

profile of v2, /device:TPU:8, one launch (start us, length us, event | category | flops | bytes accessed | tf_op | source)
XLA Modules:
  0.0 229.9 jit_solution(5089623746157346574)
XLA Ops:
  0.6 0.0 copy-start.4
  0.6 0.0 copy-start.5
  0.7 0.0 copy-start.3
  0.7 0.0 copy-start.2
  0.7 0.0 copy-start
  0.7 0.0 copy-start.6
  0.7 2.2 fusion
  3.0 0.0 copy-done.4
  3.0 0.3 fusion.6
  3.3 0.0 copy-done.5
  3.3 0.1 select_reduce_fusion
  3.4 0.6 fusion.7
  4.1 0.6 pad_maximum_fusion.1.spread
  4.7 0.0 copy-done.2
  4.7 0.2 copy.21
  4.9 0.0 copy-done.3
  4.9 0.2 copy.22
  5.0 1.1 pad_maximum_fusion.pairs
  6.2 0.0 copy-done
  6.2 0.0 copy-done.6
  6.2 2.8 %convolution_convert_fusion.1.ordered = bf16[512,2048]{1,0:T(8,128)(2,1)} fusion(bf16[512,2048]{1,0:T(8,128)(2,1)S(1)} %copy-done, f32[2048]{0:T(1024)S(1)} %copy-done.6, f32[512]{0:T(512)S(1)} %add_rsqrt_fusion, s32[512]{0:T(512)S(1)} %fusion.19), kind=kOutput, calls=%fused_computation.6 | convolution fusion | flops 1079246848 | bytes 4206592 | tf_op jit(solution)/shard_map/dot_general | solution.py:677
  9.0 215.7 %shard_map.140 = (bf16[512,2048]{1,0:T(8,128)(2,1)}, bf16[256,2048]{1,0:T(8,128)(2,1)}) custom-call(bf16[512,2048]{1,0:T(8,128)(2,1)} %convolution_convert_fusion.1.ordered, f32[2,4,8,128]{3,2,1,0:T(8,128)} %pad_maximum_fusion.1.spread, bf16[4,2048,256]{2,1,0:T(8,128)(2,1)} %gate.1, bf16[4,2048,256]{2,1,0:T(8,128)(2,1)} %up.1, bf16[4,2048,256]{2,1,0:T(8,128)(2,1)} %down.1, ...), custom_call_target="tpu_custom_call" | custom-call | flops 51539607552 | bytes 12582912 | tf_op jit(solution)/shard_map/pallas_call | solution.py:614
  224.6 0.0 copy-start.1
  224.6 4.3 %convolution_convert_fusion = bf16[512,2048]{1,0:T(8,128)(2,1)} fusion(bf16[512,2048]{1,0:T(8,128)(2,1)} %get-tuple-element.5, s32[512]{0:T(512)S(1)} %bitcast.19), kind=kOutput, calls=%fused_computation.5 | convolution fusion | flops 1075052544 | bytes 4196352 | tf_op jit(solution)/shard_map/dot_general | solution.py:694
  228.9 0.0 copy-done.1
  228.9 1.0 copy.26
  (10 shorter events, 0.1 us)
Async XLA Ops:
  0.6 2.3 %copy-start.4 = (s32[512,2]{0,1:T(2,128)S(1)}, s32[512,2]{0,1:T(2,128)}, u32[]{:S(2)}) copy-start(s32[512,2]{0,1:T(2,128)} %param.20) | copy-start | bytes 12292
  0.6 2.7 %copy-start.5 = (f32[512,2]{0,1:T(2,128)S(1)}, f32[512,2]{0,1:T(2,128)}, u32[]{:S(2)}) copy-start(f32[512,2]{0,1:T(2,128)} %param.21) | copy-start | bytes 12292
  0.7 4.2 %copy-start.3 = (bf16[1024,64]{0,1:T(8,128)(2,1)S(1)}, bf16[1024,64]{0,1:T(8,128)(2,1)}, u32[]{:S(2)}) copy-start(bf16[1024,64]{0,1:T(8,128)(2,1)} %param.15) | copy-start | bytes 393220
  0.7 4.0 %copy-start.2 = (bf16[1024,64]{0,1:T(8,128)(2,1)S(1)}, bf16[1024,64]{0,1:T(8,128)(2,1)}, u32[]{:S(2)}) copy-start(bf16[1024,64]{0,1:T(8,128)(2,1)} %param.14) | copy-start | bytes 393220
  0.7 5.5 %copy-start = (bf16[512,2048]{1,0:T(8,128)(2,1)S(1)}, bf16[512,2048]{1,0:T(8,128)(2,1)}, u32[]{:S(2)}) copy-start(bf16[512,2048]{1,0:T(8,128)(2,1)} %param.19) | copy-start | bytes 6291460
  0.7 5.5 %copy-start.6 = (f32[2048]{0:T(1024)S(1)}, f32[2048]{0:T(1024)}, u32[]{:S(2)}) copy-start(f32[2048]{0:T(1024)} %param.22) | copy-start | bytes 24580
  224.6 4.3 %copy-start.1 = (bf16[256,2048]{1,0:T(8,128)(2,1)S(1)}, bf16[256,2048]{1,0:T(8,128)(2,1)}, u32[]{:S(2)}) copy-start(bf16[256,2048]{1,0:T(8,128)(2,1)} %get-tuple-element.12) | copy-start | bytes 3145732

commit v3 on v2

--- a/solution.py
+++ b/solution.py
@@ -184,19 +184,23 @@
 MESH = pl.DeviceIdType.MESH
 QUAD = 4
 PART_ROWS = 64
+LAG = 3
+DEPTH = 1
 
 
 def fused_layer(steps, rows, ordered, spread, gate, up, down, queries, pairs, sinks, out_weight,
                 out_gain, out, mixer_out,
                 xbuf, wraw, wcol, wg, wu, wd, hid, own, part, got1, got2, fin,
                 held_queries, band, mine, theirs, wo, mixed, stage,
-                send, recv, wsem, ssem, asem):
+                send, recv, wsem, ssem, asem, wosem):
     plane, member, place = (lax.axis_index(a) for a in ("group", "member", "tp"))
     experts, width, units = gate.shape
     share = spread.shape[-1]
     here = experts * units
     blocks = 2 * experts
     first = rows // 2
+    early = rows * 3 // 4 // 16 * 16
+    wo_rows = out_weight.shape[0] // steps
     sequence_rows = queries.shape[0]
     heads_here = queries.shape[1] // HEAD_DIM
     lanes = 2 * HEAD_DIM
@@ -240,13 +244,13 @@
 
     def pass_y(s):
         return remote(
-            xbuf.at[s, slot(1, 0, first)], xbuf.at[s, slot(3, 0, first)], s, 3, device(dy=1)
+            xbuf.at[s, slot(1, 0, early)], xbuf.at[s, slot(3, 0, early)], s, 3, device(dy=1)
         )
 
     def pass_x(s):
         return remote(
-            xbuf.at[s, slot(2, first, rows - first)],
-            xbuf.at[s, slot(3, first, rows - first)], s, 4, device(dx=1),
+            xbuf.at[s, slot(2, early, rows - early)],
+            xbuf.at[s, slot(3, early, rows - early)], s, 4, device(dx=1),
         )
 
     def corner_x(s):
@@ -325,8 +329,19 @@
     queries_in = pltpu.make_async_copy(queries, held_queries, asem.at[2, 1])
     wo_own = pltpu.make_async_copy(out_weight, wo.at[0], asem.at[2, 2])
     wo_core = attention_remote(out_weight, wo.at[1], 2, device(dcore=1))
-    wo_across = attention_remote(out_weight, wo.at[2], 3, device(dx=1))
-    wo_pass = attention_remote(wo.at[2], wo.at[3], 4, device(dcore=1))
+
+    def wo_piece(src, k, n, target):
+        piece = pl.ds(pl.multiple_of(n * wo_rows, 16), wo_rows)
+        return pltpu.make_async_remote_copy(
+            src_ref=src.at[piece], dst_ref=wo.at[k, piece], send_sem=wosem.at[k - 2, n],
+            recv_sem=wosem.at[k, n], device_id=target, device_id_type=MESH,
+        )
+
+    def wo_across(n):
+        return wo_piece(out_weight, 2, n, device(dx=1))
+
+    def wo_pass(n):
+        return wo_piece(wo.at[2], 3, n, device(dcore=1))
 
     def attended_to(k):
         dx, dcore = k // 2, k % 2
@@ -382,7 +397,11 @@
             attended_to(k).wait_recv()
         wo_own.wait()
         wo_core.wait_recv()
-        wo_pass.wait_recv()
+
+        @pl.loop(0, steps)
+        def _(n):
+            wo_pass(n).wait_recv()
+
         start = pl.multiple_of(place * token_rows, 16)
         step = 256
 
@@ -420,37 +439,43 @@
     for s in range(steps):
         if far(s) == 0:
             local_in(s).start()
-    for s in range(steps):
+    def gather(s):
+        @pl.when(far(s) == 0)
+        def _():
+            local_in(s).wait()
+
+        @pl.when(far(s) != 0)
+        def _():
+            dispatch(s).wait_recv()
+
+        to_x(s).start()
+        to_y(s).start()
+        more = s + DEPTH
+
+        @pl.when(jnp.logical_and(more < steps, far(more) != 0))
+        def _():
+            dispatch(more).start()
+
+    def forward(s):
+        to_x(s).wait_recv()
+        pass_y(s).start()
+        to_y(s).wait_recv()
+        pass_x(s).start()
+
+    for s in range(1, DEPTH):
         if far(s) != 0:
             dispatch(s).start()
+    gather(0)
     for copy in (band_low, band_high, band_own, queries_in):
         copy.start()
     for copy in spread_copies():
         copy.start()
     for copy in weight_copies():
         copy.start()
-    for copy in (wo_own, wo_core, wo_across):
+    for copy in (wo_own, wo_core):
         copy.start()
-
-    def gather(s):
-        @pl.when(far(s) == 0)
-        def _():
-            local_in(s).wait()
-
-        @pl.when(far(s) != 0)
-        def _():
-            dispatch(s).wait_recv()
-
-        to_x(s).start()
-        to_y(s).start()
-
-    def forward(s):
-        to_x(s).wait_recv()
-        pass_y(s).start()
-        to_y(s).wait_recv()
-        pass_x(s).start()
-
-    gather(0)
+    wo_across(0).start()
+    wo_across(1).start()
     band_own.wait()
     queries_in.wait()
     band_low.wait_recv()
@@ -474,8 +499,6 @@
 
     for k in range(1, 4):
         attended_to(k).start()
-    wo_across.wait_recv()
-    wo_pass.start()
 
     for copy in spread_copies():
         if hasattr(copy, "wait_recv") and copy.is_remote:
@@ -511,7 +534,7 @@
                 hid[...], wd[columns, :], (((1,), (1,)), ((), ())),
                 preferred_element_type=jnp.float32,
             )
-            own[s % 3, :, columns] = p[:rows]
+            own[s % LAG, :, columns] = p[:rows]
             part[s, :, columns] = p[rows:].astype(jnp.bfloat16)
 
     def settle(s):
@@ -530,7 +553,7 @@
         sum_y(s).wait_recv()
         sum_x(s).wait_recv()
         fin[s] = (
-            own[s % 3] + got2[s, :rows].astype(jnp.float32) + got2[s, rows:].astype(jnp.float32)
+            own[s % LAG] + got2[s, :rows].astype(jnp.float32) + got2[s, rows:].astype(jnp.float32)
         ).astype(jnp.bfloat16)
 
         @pl.when(far(s) == 0)
@@ -541,19 +564,21 @@
         def _():
             give_back(s).start()
 
-    @pl.loop(0, steps + 2)
+    @pl.loop(0, steps + LAG - 1)
     def _(i):
         @pl.when(i + 2 < steps)
         def _():
             forward(i + 2)
+            wo_across(i + 2).start()
 
         @pl.when(i + 3 < steps)
         def _():
             gather(i + 3)
 
-        @pl.when(i >= 2)
-        def _():
-            finish(i - 2)
+        @pl.when(jnp.logical_and(i >= 1, i <= steps))
+        def _():
+            wo_across(i - 1).wait_recv()
+            wo_pass(i - 1).start()
 
         @pl.when(i < steps)
         def _():
@@ -563,18 +588,22 @@
             corner_x(i).start()
             corner_y(i).start()
 
-        @pl.when(jnp.logical_and(i >= 1, i < steps + 1))
+        @pl.when(jnp.logical_and(i >= 1, i <= steps))
         def _():
             settle(i - 1)
 
-        @pl.when(i == steps // 2)
+        @pl.when(i >= LAG - 1)
+        def _():
+            finish(i - LAG + 1)
+
+        @pl.when(i == steps)
         def _():
             project_rows()
 
     mixer_done.wait()
     for k in range(1, 4):
         attended_to(k).wait_send()
-    for copy in (band_low, band_high, wo_core, wo_across, wo_pass):
+    for copy in (band_low, band_high, wo_core):
         copy.wait_send()
     for copy in spread_copies():
         if copy.is_remote:
@@ -585,7 +614,9 @@
 
     @pl.loop(0, steps)
     def _(s):
-        for copy in (to_x, to_y, pass_y, pass_x, corner_x, corner_y, sum_x, sum_y):
+        for copy in (
+            to_x, to_y, pass_y, pass_x, corner_x, corner_y, sum_x, sum_y, wo_across, wo_pass
+        ):
             copy(s).wait_send()
 
         @pl.when(far(s) == 0)
@@ -627,7 +658,7 @@
             pltpu.VMEM((2 * experts, width, units), jnp.bfloat16),
             pltpu.VMEM((width, hidden), jnp.bfloat16),
             pltpu.VMEM((QUAD * rows, hidden), jnp.bfloat16),
-            pltpu.VMEM((3, rows, width), jnp.float32),
+            pltpu.VMEM((LAG, rows, width), jnp.float32),
             pltpu.VMEM((steps, (QUAD - 1) * rows, width), jnp.bfloat16),
             pltpu.VMEM((steps, rows, width), jnp.bfloat16),
             pltpu.VMEM((steps, 2 * rows, width), jnp.bfloat16),
@@ -644,6 +675,7 @@
             dma((3, 3 * experts)),
             dma((2, GROUPS * QUAD)),
             dma((3, 8)),
+            dma((4, steps)),
         ],
         compiler_params=pltpu.CompilerParams(
             collective_id=0, has_side_effects=True, vmem_limit_bytes=66 * 10**6

time: 230 us -> 190 us (0.83)
  Pallas kernels: 216 us -> 175 us
    pallas_call x1, Pallas kernels: 216 us -> 175 us  [apply_fused(): pl.pallas_call(functools.partial(fused_layer, steps, rows), out_shape=(ja...]
where the time goes in v3:
time: 190 us; the launch traced here: 189 us
  Pallas kernels  175 us (92%)
  matrix products  7.94 us (4%)
  other arithmetic  4.16 us (2%)
    pallas_call x1, Pallas kernels, apply_fused(): pl.pallas_call(functools.partial(fused_layer, steps, rows), out_shape=(ja...  175 us
    dot_general x1, matrix products, layer_fused(): jnp.dot(back, result, preferred_element_type=jnp.float32)  4.3 us

profile of v3, /device:TPU:8, one launch (start us, length us, event | category | flops | bytes accessed | tf_op | source)
XLA Modules:
  0.0 189.4 jit_solution(4332726448484274116)
XLA Ops:
  0.6 0.0 copy-start.4
  0.6 0.0 copy-start.5
  0.7 0.0 copy-start.3
  0.7 0.0 copy-start.2
  0.7 0.0 copy-start
  0.7 0.0 copy-start.6
  0.7 2.2 %fusion = f32[512]{0:T(512)S(1)} fusion(bf16[512,2048]{1,0:T(8,128)(2,1)} %param.19), kind=kLoop, calls=%fused_computation.2 | loop fusion | flops 3145216 | bytes 2099200 | tf_op jit(solution)/shard_map/reduce_sum | solution.py:698
  3.0 0.0 copy-done.4
  3.0 0.3 fusion.6
  3.3 0.0 copy-done.5
  3.3 0.1 select_reduce_fusion
  3.4 0.6 fusion.7
  4.1 0.6 pad_maximum_fusion.1.spread
  4.7 0.0 copy-done.2
  4.7 0.2 copy.21
  4.9 0.0 copy-done.3
  4.9 0.2 copy.22
  5.0 1.1 pad_maximum_fusion.pairs
  6.2 0.0 copy-done
  6.2 0.0 copy-done.6
  6.2 2.8 %convolution_convert_fusion.1.ordered = bf16[512,2048]{1,0:T(8,128)(2,1)} fusion(bf16[512,2048]{1,0:T(8,128)(2,1)S(1)} %copy-done, f32[2048]{0:T(1024)S(1)} %copy-done.6, f32[512]{0:T(512)S(1)} %add_rsqrt_fusion, s32[512]{0:T(512)S(1)} %fusion.19), kind=kOutput, calls=%fused_computation.6 | convolution fusion | flops 1079246848 | bytes 4206592 | tf_op jit(solution)/shard_map/dot_general | solution.py:709
  9.0 175.1 %shard_map.140 = (bf16[512,2048]{1,0:T(8,128)(2,1)}, bf16[256,2048]{1,0:T(8,128)(2,1)}) custom-call(bf16[512,2048]{1,0:T(8,128)(2,1)} %convolution_convert_fusion.1.ordered, f32[2,4,8,128]{3,2,1,0:T(8,128)} %pad_maximum_fusion.1.spread, bf16[4,2048,256]{2,1,0:T(8,128)(2,1)} %gate.1, bf16[4,2048,256]{2,1,0:T(8,128)(2,1)} %up.1, bf16[4,2048,256]{2,1,0:T(8,128)(2,1)} %down.1, ...), custom_call_target="tpu_custom_call" | custom-call | flops 51539607552 | bytes 12582912 | tf_op jit(solution)/shard_map/pallas_call | solution.py:645
  184.1 0.0 copy-start.1
  184.1 4.3 %convolution_convert_fusion = bf16[512,2048]{1,0:T(8,128)(2,1)} fusion(bf16[512,2048]{1,0:T(8,128)(2,1)} %get-tuple-element.5, s32[512]{0:T(512)S(1)} %bitcast.19), kind=kOutput, calls=%fused_computation.5 | convolution fusion | flops 1075052544 | bytes 4196352 | tf_op jit(solution)/shard_map/dot_general | solution.py:726
  188.4 0.0 copy-done.1
  188.4 1.0 copy.26
  (10 shorter events, 0.1 us)
Async XLA Ops:
  0.6 2.3 %copy-start.4 = (s32[512,2]{0,1:T(2,128)S(1)}, s32[512,2]{0,1:T(2,128)}, u32[]{:S(2)}) copy-start(s32[512,2]{0,1:T(2,128)} %param.20) | copy-start | bytes 12292
  0.6 2.7 %copy-start.5 = (f32[512,2]{0,1:T(2,128)S(1)}, f32[512,2]{0,1:T(2,128)}, u32[]{:S(2)}) copy-start(f32[512,2]{0,1:T(2,128)} %param.21) | copy-start | bytes 12292
  0.7 4.2 %copy-start.3 = (bf16[1024,64]{0,1:T(8,128)(2,1)S(1)}, bf16[1024,64]{0,1:T(8,128)(2,1)}, u32[]{:S(2)}) copy-start(bf16[1024,64]{0,1:T(8,128)(2,1)} %param.15) | copy-start | bytes 393220
  0.7 4.0 %copy-start.2 = (bf16[1024,64]{0,1:T(8,128)(2,1)S(1)}, bf16[1024,64]{0,1:T(8,128)(2,1)}, u32[]{:S(2)}) copy-start(bf16[1024,64]{0,1:T(8,128)(2,1)} %param.14) | copy-start | bytes 393220
  0.7 5.5 %copy-start = (bf16[512,2048]{1,0:T(8,128)(2,1)S(1)}, bf16[512,2048]{1,0:T(8,128)(2,1)}, u32[]{:S(2)}) copy-start(bf16[512,2048]{1,0:T(8,128)(2,1)} %param.19) | copy-start | bytes 6291460
  0.7 5.5 %copy-start.6 = (f32[2048]{0:T(1024)S(1)}, f32[2048]{0:T(1024)}, u32[]{:S(2)}) copy-start(f32[2048]{0:T(1024)} %param.22) | copy-start | bytes 24580
  184.1 4.3 %copy-start.1 = (bf16[256,2048]{1,0:T(8,128)(2,1)S(1)}, bf16[256,2048]{1,0:T(8,128)(2,1)}, u32[]{:S(2)}) copy-start(bf16[256,2048]{1,0:T(8,128)(2,1)} %get-tuple-element.12) | copy-start | bytes 3145732
